TPU v7x, 32 devices: a whole 2x2x4 slice. The times are simulated.
32 devices in a mesh: grp: 2 (over x), ep: 16 (over z, y, core), tp: 1.
Axes of the slice: x: 2, y: 2, z: 4, core: 2. Of those that a mesh axis runs over, the one named last changes fastest.
Arguments:
- tokens: bfloat16 [2048, 2048], P(('grp', 'ep')), parts along dimension 0, may hold values from -6 to 6
- norm_gain: float32 [2048], replicated, may hold values from 0.1 to 1.9
- expert_gate: bfloat16 [16, 2048, 512], P('ep', None, 'tp'), may hold values from -0.125 to 0.125
- expert_up: bfloat16 [16, 2048, 512], P('ep', None, 'tp'), may hold values from -0.125 to 0.125
- expert_down: bfloat16 [16, 512, 2048], P('ep', 'tp'), may hold values from -0.25 to 0.25
- shared_gate: bfloat16 [2048, 512], P(None, 'tp'), may hold values from -0.125 to 0.125
- shared_up: bfloat16 [2048, 512], P(None, 'tp'), may hold values from -0.125 to 0.125
- shared_down: bfloat16 [512, 2048], P('tp'), may hold values from -0.25 to 0.25
- routes: int32 [2048, 8], P(('grp', 'ep')), parts along dimension 0, may hold values from 0 to 15, all different within a row; in each aligned block of 64 rows (0 to 63, 64 to 127, ...) at most 64 rows name the same one
- route_weights: float32 [2048, 8], P(('grp', 'ep')), parts along dimension 0, may hold values from 0.05 to 0.6
Outputs:
- mixed: bfloat16 [2048, 2048], P(('grp', 'ep'), 'tp'), parts along dimension 0
There are 2 independent parts, one for each index of `grp`. A program takes and returns all parts, laid end to end along the dimension named above; an argument that names none is the same for every part. Nothing has to cross between parts.
Inputs may be any that keep to these rules, and one draw needn't show every extreme that they name: `routes`: each row names 8 different experts. Within the rows of one index of ep no expert is named more than 64 times, a bound that some block reaches by the rows of some index of ep.
All inputs are finite; a program needn't handle non-finite values.
Results may differ from a plain program's by a relative error of at most 0.0085.
Values may be sent and summed in bfloat16 or wider, within the bound.
A program may use at most 64 MiB of HBM per device.

v0:
```python
import jax
import jax.numpy as jnp
from jax import lax
from jax.sharding import PartitionSpec as P


def rms_scaled(values, gain):
    wide = values.astype(jnp.float32)
    scaled = wide * lax.rsqrt(jnp.mean(wide * wide, axis=-1, keepdims=True) + 1e-06)
    return (scaled * gain).astype(jnp.bfloat16)


def swiglu_partial(row_block, w_gate, w_up, w_down):
    gate_proj = jnp.dot(row_block, w_gate, preferred_element_type=jnp.float32)
    up_proj = jnp.dot(row_block, w_up, preferred_element_type=jnp.float32)
    hidden = (jax.nn.silu(gate_proj) * up_proj).astype(jnp.bfloat16)
    partial_value = jnp.dot(hidden, w_down, preferred_element_type=jnp.float32)
    return lax.optimization_barrier(partial_value.astype(jnp.bfloat16)).astype(jnp.float32)


def per_device(
    tokens,
    norm_gain,
    expert_gate,
    expert_up,
    expert_down,
    shared_gate,
    shared_up,
    shared_down,
    routes,
    route_weights,
):
    tok_rows = tokens.shape[0]
    model_width = tokens.shape[1]
    top_count = routes.shape[1]
    experts = lax.axis_size("ep")
    half_width = model_width // lax.axis_size("tp")
    capacity = min(tok_rows, 2 * tok_rows * top_count // experts)
    normed = rms_scaled(tokens, norm_gain)
    shared_part = swiglu_partial(normed, shared_gate, shared_up, shared_down)
    all_normed = lax.all_gather(normed, "ep", axis=0, tiled=True)
    all_routes = lax.all_gather(routes, "ep", axis=0, tiled=True)
    all_weights = lax.all_gather(route_weights, "ep", axis=0, tiled=True)
    own_expert = lax.axis_index("ep")
    hit_table = all_routes == own_expert
    is_mine = jnp.sum(hit_table.astype(jnp.int32), axis=1).reshape(experts, tok_rows)
    weight_mine = jnp.sum(jnp.where(hit_table, all_weights, jnp.float32(0.0)), axis=1).reshape(
        experts, tok_rows
    )
    slot_rank = jnp.cumsum(is_mine, axis=1) - is_mine
    matches = (slot_rank[:, None, :] == jnp.arange(capacity, dtype=jnp.int32)[None, :, None]) & (
        is_mine[:, None, :] == 1
    )
    slot_token = jnp.sum(
        jnp.where(matches, jnp.arange(tok_rows, dtype=jnp.int32)[None, None, :], 0), axis=2
    )
    slot_live = jnp.any(matches, axis=2).reshape(-1)
    slot_weight = jnp.sum(
        jnp.where(matches, weight_mine[:, None, :], jnp.float32(0.0)), axis=2
    ).reshape(-1)
    global_row = (jnp.arange(experts, dtype=jnp.int32)[:, None] * tok_rows + slot_token).reshape(-1)
    taken = jnp.take(all_normed, global_row, axis=0)
    inbound = jnp.where(slot_live[:, None], taken, jnp.zeros_like(taken))
    expert_part = swiglu_partial(inbound, expert_gate[0], expert_up[0], expert_down[0])
    expert_sum, shared_sum = (
        lax.psum_scatter(
            expert_part.astype(jnp.bfloat16), "tp", scatter_dimension=1, tiled=True
        ).astype(jnp.float32),
        lax.psum_scatter(
            shared_part.astype(jnp.bfloat16), "tp", scatter_dimension=1, tiled=True
        ).astype(jnp.float32),
    )
    expert_out = expert_sum.astype(jnp.bfloat16)
    shared_out = shared_sum.astype(jnp.bfloat16)
    weighted_rows = expert_out.astype(jnp.float32) * slot_weight[:, None]
    terms = (
        jnp.zeros((experts * tok_rows, half_width), jnp.float32).at[global_row].add(weighted_rows)
    )
    routed = lax.psum_scatter(terms, "ep", scatter_dimension=0, tiled=True)
    return (routed + shared_out.astype(jnp.float32)).astype(jnp.bfloat16)


def solution(mesh):
    in_specs = (
        P(("grp", "ep"), None),
        P(),
        P("ep", None, "tp"),
        P("ep", None, "tp"),
        P("ep", "tp", None),
        P(None, "tp"),
        P(None, "tp"),
        P("tp", None),
        P(("grp", "ep"), None),
        P(("grp", "ep"), None),
    )
    out_specs = P(("grp", "ep"), "tp")
    return jax.shard_map(
        per_device, mesh=mesh, in_specs=in_specs, out_specs=out_specs, check_vma=False
    )
```

profile of v0, /device:TPU:0, one launch (start us, length us, event | category | flops | bytes accessed | tf_op | source)
XLA Modules:
  0.0 220.2 jit_solution(10762716393236686828)
XLA Ops:
  6.5 0.0 copy-start
  6.5 0.0 all-gather.4.cloned.1.call-start
  6.5 1.2 fusion.15
  7.8 1.8 fusion.17
  9.6 0.0 all-gather.4.cloned.1.call-update
  9.6 0.0 reduce-scatter.2.cloned.1.call-start
  9.7 23.8 %all-gather = s32[16,64,8]{1,2,0:T(8,128)S(1)} all-gather(s32[1,64,8]{1,2,0:T(8,128)} %bitcast.23), channel_id=1, replica_groups=mesh['grp'=2,'ep'=16,'tp'=1] {'ep'}, dimensions={0}, use_global_device_ids=true | all-gather | bytes 34816 | tf_op jit(solution)/shard_map/all_gather | solution.py:42
  33.4 18.4 %all-gather.1 = f32[16,64,8]{1,2,0:T(8,128)S(1)} all-gather(f32[1,64,8]{1,2,0:T(8,128)} %bitcast.24), channel_id=1, replica_groups=mesh['grp'=2,'ep'=16,'tp'=1] {'ep'}, dimensions={0}, use_global_device_ids=true | all-gather | bytes 34816 | tf_op jit(solution)/shard_map/all_gather | solution.py:43
  51.9 0.2 reduce_window_sum.14
  52.1 0.4 select_reduce_fusion.1
  52.5 0.1 broadcast_add_fusion
  52.5 0.1 add.80
  52.6 0.1 add.77
  52.7 0.2 select_reduce_fusion
  52.9 0.1 mul.59
  53.0 0.4 fusion.19
  53.3 0.1 broadcast_in_dim.66
  53.5 9.7 %all-gather.4.cloned.1.call-done = bf16[1024,2048]{1,0:T(8,128)(2,1)} async-done(((bf16[64,2048]{1,0:T(8,128)(2,1)}), bf16[1024,2048]{1,0:T(8,128)(2,1)}) %all-gather.4.cloned.1.call-update) | async-done | bytes 4194320 | tf_op jit(solution)/shard_map/all_gather | solution.py:41
  63.2 11.7 %gather_fusion = bf16[1024,2048]{1,0:T(8,128)(2,1)} fusion(bf16[1024,2048]{1,0:T(8,128)(2,1)} %all-gather.4.cloned.1.call-done, s32[1024]{0:T(1024)S(1)} %broadcast_clamp_fusion), kind=kCustom, calls=%fused_computation | custom fusion | bytes 8392704 | tf_op jit(solution)/shard_map/jit(_take)/gather | solution.py:62
  75.0 6.6 %fusion.6 = f32[1024,512]{1,0:T(8,128)} fusion(bf16[1,2048,512]{2,1,0:T(8,128)(2,1)} %param.13, bf16[1024,2048]{1,0:T(8,128)(2,1)} %gather_fusion, pred[1024]{0:T(1024)(128)(4,1)S(1)} %compare_and_fusion, pred[1024]{0:T(1024)(128)(4,1)S(1)} %broadcast_in_dim.66), kind=kOutput, calls=%fused_computation.11 | convolution fusion | flops 2151677952 | bytes 8390656 | tf_op jit(solution)/shard_map/dot_general | solution.py:15
  81.5 0.0 copy-done
  81.5 9.2 %convolution_convert_fusion = bf16[1024,2048]{1,0:T(8,128)(2,1)} fusion(bf16[1,512,2048]{2,1,0:T(8,128)(2,1)S(1)} %copy-done, f32[1024,512]{1,0:T(8,128)} %fusion.6, bf16[1,2048,512]{2,1,0:T(8,128)(2,1)} %param.12, bf16[1024,2048]{1,0:T(8,128)(2,1)} %gather_fusion, pred[1024]{0:T(1024)(128)(4,1)S(1)} %compare_and_fusion, ...), kind=kOutput, calls=%fused_computation.8 | convolution fusion | flops 4304404480 | bytes 14682112 | tf_op jit(solution)/shard_map/dot_general | solution.py:17
  90.7 18.6 %scatter_custom_fusion = f32[1024,2048]{1,0:T(8,128)} fusion(s32[1024]{0:T(1024)S(1)} %bitcast.22, bf16[1024,2048]{1,0:T(8,128)(2,1)} %convolution_convert_fusion, f32[1024]{0:T(1024)S(1)} %mul.59, f32[]{:T(128)} %constant.13.clone.1), kind=kCustom, calls=%fused_computation.2 | custom fusion | flops 6291456 | bytes 12587012 | tf_op jit(solution)/shard_map/scatter-add | solution.py:77
  109.3 0.0 copy-start.1
  109.3 0.0 reduce-scatter.2.cloned.1.call-update
  109.4 0.9 copy-done.1
  110.3 2.1 fusion.28
  112.4 3.5 %convolution_convert_fusion.1 = bf16[64,2048]{1,0:T(8,128)(2,1)S(1)} fusion(bf16[512,2048]{1,0:T(8,128)(2,1)} %param.17, bf16[64,2048]{1,0:T(8,128)(2,1)S(1)} %copy-done.1, bf16[2048,512]{1,0:T(8,128)(2,1)} %param.16, f32[64,512]{1,0:T(8,128)S(1)} %fusion.28), kind=kOutput, calls=%fused_computation.9 | convolution fusion | flops 268763136 | bytes 4849664 | tf_op jit(solution)/shard_map/dot_general | solution.py:17
  115.9 95.8 %reduce-scatter.2.cloned.1.call-done = f32[64,2048]{1,0:T(8,128)} async-done(((f32[1024,2048]{1,0:T(8,128)}), f32[64,2048]{1,0:T(8,128)}) %reduce-scatter.2.cloned.1.call-update) | async-done | bytes 524304 | tf_op jit(solution)/shard_map/reduce_scatter | solution.py:79
  211.6 1.8 add_convert_fusion
  (9 shorter events, 0.1 us)
Async XLA Ops:
  6.5 75.0 %copy-start = (bf16[1,512,2048]{2,1,0:T(8,128)(2,1)S(1)}, bf16[1,512,2048]{2,1,0:T(8,128)(2,1)}, u32[]{:S(2)}) copy-start(bf16[1,512,2048]{2,1,0:T(8,128)(2,1)} %param.14) | copy-start | bytes 6291460
  6.5 56.7 %all-gather.4.cloned.1.call-start = ((), (), s32[]{:S(2)}) async-start(), calls=%async_computation.1 | async-start | bytes 4456448 | tf_op jit(solution)/shard_map/all_gather | solution.py:41
  9.6 202.0 %reduce-scatter.2.cloned.1.call-start = ((), (), s32[]{:S(2)}) async-start(), calls=%async_computation.2 | async-start | bytes 8912896 | tf_op jit(solution)/shard_map/reduce_scatter | solution.py:79
  109.3 0.9 copy-start.1
Sparse Core Ops, SparseCore 0:
  9.7 53.4 all-gather.3
  109.5 102.0 reduce-scatter.1
where the time goes:
time: 221 us; the launch traced here: 220 us
  waiting for transfers between devices  106 us (48%)
  blocking collectives  42.1 us (19%)
  other arithmetic  24.8 us (11%)
  matrix products  21.3 us (10%)
  between operations  13.5 us (6%)
  local copies, waits for them, and re-layouts  13 us (6%)
    reduce_scatter x1, waiting for transfers between devices, per_device(): routed = lax.psum_scatter(terms, 'ep', scatter_dimension=0, tiled=True)  95.8 us
    all_gather x1, blocking collectives, per_device(): all_routes = lax.all_gather(routes, 'ep', axis=0, tiled=True)  23.8 us
    scatter-add x1, other arithmetic, per_device(): jnp.zeros((experts * tok_rows, half_width), jnp.float32).at[global_row]  18.6 us
    all_gather x1, blocking collectives, per_device(): all_weights = lax.all_gather(route_weights, 'ep', axis=0, tiled=True)  18.4 us
    dot_general x2, matrix products, swiglu_partial(): partial_value = jnp.dot(hidden, w_down, preferred_element_type=jnp.float32)  12.7 us
    gather x1, local copies, waits for them, and re-layouts, per_device(): taken = jnp.take(all_normed, global_row, axis=0)  11.7 us
    all_gather x1, waiting for transfers between devices, per_device(): all_normed = lax.all_gather(normed, 'ep', axis=0, tiled=True)  9.75 us
    dot_general x1, matrix products, swiglu_partial(): up_proj = jnp.dot(row_block, w_up, preferred_element_type=jnp.float32)  6.57 us
  transfers between devices with their start and end apart: 2, of which 2 were waited for; matrix products, arithmetic and copies ran while one was open for 3% of the time, Pallas kernels for 0%

commit v1 on v0

--- a/solution.py
+++ b/solution.py
@@ -1,6 +1,10 @@
+import functools
+
 import jax
 import jax.numpy as jnp
 from jax import lax
+from jax.experimental import pallas as pl
+from jax.experimental.pallas import tpu as pltpu
 from jax.sharding import PartitionSpec as P
 
 
@@ -80,6 +84,345 @@
     return (routed + shared_out.astype(jnp.float32)).astype(jnp.bfloat16)
 
 
+RING_SENDS = ((3, 1, None), (4, 0, None), (2, 1, 0), (3, 0, 1), (1, 1, 2), (2, 0, 3), (1, 0, 5))
+LAST_IN = (6, 4)
+
+
+def remote(src, dst, send_sem, recv_sem, target):
+    return pltpu.make_async_remote_copy(
+        src_ref=src,
+        dst_ref=dst,
+        send_sem=send_sem,
+        recv_sem=recv_sem,
+        device_id={"ep": target},
+        device_id_type=pl.DeviceIdType.MESH,
+    )
+
+
+def moe_kernel(
+    chips,
+    tok_ref,
+    gain_ref,
+    routes_ref,
+    rweights_ref,
+    eg_hbm,
+    eu_hbm,
+    ed_hbm,
+    sg_hbm,
+    su_hbm,
+    sd_hbm,
+    out_ref,
+    rows,
+    part,
+    mate,
+    hid,
+    eg,
+    eu,
+    ed,
+    sg,
+    su,
+    sd,
+    sbuf,
+    rbuf,
+    shared,
+    w_sem,
+    own_sem,
+    ag_send,
+    ag_recv,
+    dd_send,
+    dd_recv,
+    y_send,
+    y_recv,
+    rs_send,
+    rs_recv,
+):
+    width = tok_ref.shape[1]
+    quarter = tok_ref.shape[0] // 2
+    block = 4 * quarter
+    experts = 2 * chips
+    depth = chips // 2
+    me = lax.axis_index("ep")
+    core = me % 2
+    side = (me // 2) % 2
+    along = me // 4
+    spot = along + side * (chips - 1 - 2 * along)
+
+    def device_at(ring_spot):
+        s = lax.rem(ring_spot + chips, chips)
+        turn = s // depth
+        return (s + turn * (chips - 1 - 2 * s)) * 4 + turn * 2 + core
+
+    partner = me + 1 - 2 * core
+    ahead = (device_at(spot + 1), device_at(spot - 1))
+
+    barrier = pltpu.get_barrier_semaphore()
+    for peer in (ahead[0], ahead[1], partner):
+        pl.semaphore_signal(
+            barrier, inc=1, device_id={"ep": peer}, device_id_type=pl.DeviceIdType.MESH
+        )
+    loads = [
+        pltpu.make_async_copy(hbm, vmem, w_sem.at[i])
+        for i, (hbm, vmem) in enumerate(
+            (
+                (eg_hbm.at[0], eg),
+                (eu_hbm.at[0], eu),
+                (ed_hbm.at[0], ed),
+                (sg_hbm, sg),
+                (su_hbm, su),
+                (sd_hbm, sd),
+            )
+        )
+    ]
+    for load in loads:
+        load.start()
+
+    wide = tok_ref[...].astype(jnp.float32)
+    scaled = wide * lax.rsqrt(jnp.mean(wide * wide, axis=-1, keepdims=True) + 1e-06)
+    normed = (scaled * gain_ref[...]).astype(jnp.bfloat16)
+    rows[0, core, :, :, :width] = normed.reshape(2, quarter, width)
+    lane = lax.broadcasted_iota(jnp.int32, (2 * quarter, 128), 1)
+    table = jnp.zeros((2 * quarter, 128), jnp.float32)
+    for k in range(routes_ref.shape[1]):
+        table = table + jnp.where(
+            lax.rem(lane, experts) == routes_ref[:, k : k + 1], rweights_ref[:, k : k + 1], 0.0
+        )
+    coarse = table.astype(jnp.bfloat16).astype(jnp.float32)
+    table = jnp.where(lane < experts, coarse, jnp.where(lane < 2 * experts, table - coarse, 0.0))
+    rows[0, core, :, :, width:] = table.astype(jnp.bfloat16).reshape(2, quarter, 128)
+    pl.semaphore_wait(barrier, 3)
+
+    def spot_of(way, k):
+        hops = 1 + k // 2
+        half = k % 2 if way == 0 else 1 - k % 2
+        slot = 2 * hops - 1 if way == 0 else jnp.minimum(2 * hops, chips - 1)
+        return rows.at[slot, core, half]
+
+    def gather_copy(way, k, first=False):
+        half = k % 2 if way == 0 else 1 - k % 2
+        source = rows.at[0, core, half] if first else spot_of(way, k - 2)
+        return remote(
+            source, spot_of(way, k), ag_send.at[way, k], ag_recv.at[way, k], ahead[way]
+        )
+
+    def arrival(way, k):
+        ref = spot_of(way, k)
+        return remote(ref, ref, ag_send.at[way, k], ag_recv.at[way, k], ahead[way])
+
+    def across_copy(way, k):
+        ref = spot_of(way, k)
+        return remote(ref, ref, dd_send.at[way, k], dd_recv.at[way, k], partner)
+
+    def mate_copy(slot):
+        return remote(
+            part.at[slot, 1 - core], mate.at[slot], y_send.at[slot], y_recv.at[slot], partner
+        )
+
+    for k in (0, 1):
+        for way in (0, 1):
+            gather_copy(way, k, True).start()
+    own_copy = remote(rows.at[0, core], rows.at[0, core], own_sem.at[0], own_sem.at[1], partner)
+    own_copy.start()
+
+    step = 256
+
+    def hidden_of(x, gate, up, count):
+        for lower in range(0, gate.shape[1], step):
+            g = jnp.dot(x, gate[:, lower : lower + step], preferred_element_type=jnp.float32)
+            u = jnp.dot(x, up[:, lower : lower + step], preferred_element_type=jnp.float32)
+            hid[:count, lower : lower + step] = (jax.nn.silu(g) * u).astype(jnp.bfloat16)
+
+    def expert_block(slot):
+        x = rows[slot, :, :, :, :width].reshape(block, width)
+        extra = rows[slot, :, :, :, width:].reshape(block, 128).astype(jnp.float32)
+        where = lax.broadcasted_iota(jnp.int32, (block, 128), 1)
+        weight = jnp.sum(
+            jnp.where((where == me) | (where == me + experts), extra, 0.0), axis=1, keepdims=True
+        )
+        hidden_of(x, eg, eu, block)
+        for lower in range(0, width, step):
+            o = jnp.dot(
+                hid[...], ed[:, lower : lower + step], preferred_element_type=jnp.float32
+            )
+            part[slot, :, :, :, lower : lower + step] = (
+                (o * weight).astype(jnp.bfloat16).reshape(2, 2, quarter, step)
+            )
+        mate_copy(slot).start()
+
+    for load in loads[:3]:
+        load.wait()
+
+    last = chips - 2
+
+    def gather_step(u, carry):
+        for way in (0, 1):
+            arrival(way, u).wait_recv()
+
+            @pl.when(u + 2 <= last)
+            def _():
+                gather_copy(way, u + 2).start()
+
+            across_copy(way, u).start()
+
+        @pl.when(u == 0)
+        def _():
+            own_copy.wait_recv()
+
+        first = 2 * ((u + 1) // 2 - 1)
+
+        @pl.when((u > 0) & (u % 2 == 1))
+        def _():
+            across_copy(0, first).wait_recv()
+            across_copy(0, first + 1).wait_recv()
+
+        @pl.when((u > 0) & (u % 2 == 0))
+        def _():
+            across_copy(1, first).wait_recv()
+            across_copy(1, first + 1).wait_recv()
+
+        expert_block(u)
+        return carry
+
+    lax.fori_loop(0, chips - 1, gather_step, 0)
+
+    mate_seen = set()
+
+    def ring_copy(way, k):
+        return remote(
+            sbuf.at[way, k], rbuf.at[way, k], rs_send.at[way, k], rs_recv.at[way, k], ahead[way]
+        )
+
+    def ring_send(way, k):
+        hops, kind, inbound = RING_SENDS[k]
+        slot = min(2 * hops, chips - 1) if way == 0 else 2 * hops - 1
+        half = kind if way == 0 else 1 - kind
+        if slot not in mate_seen:
+            mate_copy(slot).wait_recv()
+            mate_seen.add(slot)
+        total = part[slot, core, half].astype(jnp.float32) + mate[slot, half].astype(jnp.float32)
+        if inbound is not None:
+            ring_copy(way, inbound).wait_recv()
+            total = total + rbuf[way, inbound].astype(jnp.float32)
+        sbuf[way, k] = total.astype(jnp.bfloat16)
+        ring_copy(way, k).start()
+
+    ring_send(1, 0)
+    for way in (0, 1):
+        across_copy(way, last).wait_recv()
+    expert_block(chips - 1)
+    ring_send(0, 0)
+    for way in (0, 1):
+        ring_send(way, 1)
+
+    for load in loads[3:]:
+        load.wait()
+    hidden_of(rows[0, core, :, :, :width].reshape(2 * quarter, width), sg, su, 2 * quarter)
+    mate_copy(0).wait_recv()
+    for lower in range(0, width, step):
+        o = jnp.dot(
+            hid[: 2 * quarter, :], sd[:, lower : lower + step], preferred_element_type=jnp.float32
+        )
+        cut = slice(lower, lower + step)
+        shared[:, :, cut] = (
+            o.astype(jnp.bfloat16).astype(jnp.float32).reshape(2, quarter, step)
+            + part[0, core, :, :, cut].astype(jnp.float32)
+            + mate[0, :, :, cut].astype(jnp.float32)
+        )
+
+    for k in range(2, len(RING_SENDS)):
+        for way in (0, 1):
+            ring_send(way, k)
+
+    for half in (1, 0):
+        total = shared[half]
+        for way in (0, 1):
+            k = LAST_IN[half if way == 0 else 1 - half]
+            ring_copy(way, k).wait_recv()
+            total = total + rbuf[way, k].astype(jnp.float32)
+        out_ref[half * quarter : (half + 1) * quarter, :] = total.astype(jnp.bfloat16)
+
+    own_copy.wait_send()
+    for way in (0, 1):
+        for k in range(last + 1):
+            gather_copy(way, k, k < 2).wait_send()
+            across_copy(way, k).wait_send()
+            ring_copy(way, k).wait_send()
+    for slot in range(chips):
+        mate_copy(slot).wait_send()
+
+
+def ring_per_device(
+    tokens,
+    norm_gain,
+    expert_gate,
+    expert_up,
+    expert_down,
+    shared_gate,
+    shared_up,
+    shared_down,
+    routes,
+    route_weights,
+):
+    experts = lax.axis_size("ep")
+    chips = experts // 2
+    count, width = tokens.shape
+    quarter = count // 2
+    hidden = expert_gate.shape[2]
+    half = jnp.bfloat16
+    messages = chips - 1
+    whole = pl.BlockSpec(memory_space=pltpu.VMEM)
+    stays = pl.BlockSpec(memory_space=pl.ANY)
+    dma = pltpu.SemaphoreType.DMA
+    flops = 6 * width * hidden * (experts + 1) * count
+    return pl.pallas_call(
+        functools.partial(moe_kernel, chips),
+        out_shape=jax.ShapeDtypeStruct((count, width), half),
+        in_specs=[whole] * 4 + [stays] * 6,
+        out_specs=whole,
+        scratch_shapes=[
+            pltpu.VMEM((chips, 2, 2, quarter, width + 128), half),
+            pltpu.VMEM((chips, 2, 2, quarter, width), half),
+            pltpu.VMEM((chips, 2, quarter, width), half),
+            pltpu.VMEM((2 * count, hidden), half),
+            pltpu.VMEM((width, hidden), half),
+            pltpu.VMEM((width, hidden), half),
+            pltpu.VMEM((hidden, width), half),
+            pltpu.VMEM((width, hidden), half),
+            pltpu.VMEM((width, hidden), half),
+            pltpu.VMEM((hidden, width), half),
+            pltpu.VMEM((2, messages, quarter, width), half),
+            pltpu.VMEM((2, messages, quarter, width), half),
+            pltpu.VMEM((2, quarter, width), jnp.float32),
+            dma((6,)),
+            dma((2,)),
+            dma((2, messages)),
+            dma((2, messages)),
+            dma((2, messages)),
+            dma((2, messages)),
+            dma((chips,)),
+            dma((chips,)),
+            dma((2, messages)),
+            dma((2, messages)),
+        ],
+        compiler_params=pltpu.CompilerParams(
+            collective_id=0, has_side_effects=True, vmem_limit_bytes=60 * 2**20
+        ),
+        cost_estimate=pl.CostEstimate(
+            flops=flops, bytes_accessed=12 * width * hidden, transcendentals=0
+        ),
+    )(
+        tokens,
+        norm_gain.reshape(1, width),
+        routes,
+        route_weights,
+        expert_gate,
+        expert_up,
+        expert_down,
+        shared_gate,
+        shared_up,
+        shared_down,
+    )
+
+
 def solution(mesh):
     in_specs = (
         P(("grp", "ep"), None),
@@ -94,6 +437,11 @@
         P(("grp", "ep"), None),
     )
     out_specs = P(("grp", "ep"), "tp")
+    ring = mesh.shape["tp"] == 1 and mesh.shape["ep"] == 16
     return jax.shard_map(
-        per_device, mesh=mesh, in_specs=in_specs, out_specs=out_specs, check_vma=False
-    )
+        ring_per_device if ring else per_device,
+        mesh=mesh,
+        in_specs=in_specs,
+        out_specs=out_specs,
+        check_vma=False,
+    )

time: 221 us -> 59.9 us (0.27)
  waiting for transfers between devices: 106 us -> 0 us
  Pallas kernels: 0 us -> 55.2 us
  blocking collectives: 42.1 us -> 0 us
  other arithmetic: 24.8 us -> 0 us
  matrix products: 21.3 us -> 0 us
  between operations: 13.5 us -> 0.01 us
  local copies, waits for them, and re-layouts: 13 us -> 4.42 us
    reduce_scatter x1 -> x0, waiting for transfers between devices: 95.8 us -> none  [per_device(): routed = lax.psum_scatter(terms, 'ep', scatter_dimension=0, tiled=True)]
    pallas_call x0 -> x1, Pallas kernels: none -> 55.2 us  [ring_per_device(): pl.pallas_call(functools.partial(moe_kernel, chips), out_shape=jax.ShapeD...]
    all_gather x2 -> x0, blocking collectives: 42.1 us -> none  [the longest x1 23.8 us: per_device(): all_routes = lax.all_gather(routes, 'ep', axis=0, tiled=True)]
    dot_general x4 -> x0, matrix products: 21.3 us -> none  [the longest x2 12.7 us: swiglu_partial(): partial_value = jnp.dot(hidden, w_down, preferred_element_type=jnp.float32)]
    scatter-add x1 -> x0, other arithmetic: 18.6 us -> none  [per_device(): jnp.zeros((experts * tok_rows, half_width), jnp.float32).at[global_row]]
    gather x1 -> x0, local copies, waits for them, and re-layouts: 11.7 us -> none  [per_device(): taken = jnp.take(all_normed, global_row, axis=0)]
    all_gather x1 -> x0, waiting for transfers between devices: 9.75 us -> none  [per_device(): all_normed = lax.all_gather(normed, 'ep', axis=0, tiled=True)]
    convert_element_type x2 -> x0, other arithmetic: 3.58 us -> none  [the longest x1 1.79 us: rms_scaled(): return (scaled * gain).astype(jnp.bfloat16)]
  transfers between devices with their start and end apart: 2 -> 0, of which waited for: 2 -> 0; matrix products, arithmetic and copies ran while one was open for 3% -> 0% of each run, Pallas kernels for 0% -> 0%
where the time goes in v1:
time: 59.9 us; the launch traced here: 59.6 us
  Pallas kernels  55.2 us (92%)
  local copies, waits for them, and re-layouts  4.42 us (7%)
    pallas_call x1, Pallas kernels, ring_per_device(): pl.pallas_call(functools.partial(moe_kernel, chips), out_shape=jax.ShapeD...  55.2 us
    unnamed x3, local copies, waits for them, and re-layouts  4.42 us

profile of v1, /device:TPU:0, one launch (start us, length us, event | category | flops | bytes accessed | tf_op | source)
XLA Modules:
  0.0 59.6 jit_solution(16394992655273385542)
XLA Ops:
  0.0 1.4 %copy.11.routes_ref = s32[64,8]{1,0:T(8,128)} copy(s32[64,8]{0,1:T(8,128)} %param.18) | data formatting | bytes 4096 | tf_op args[8]
  1.4 1.4 %copy.12.rweights_ref = f32[64,8]{1,0:T(8,128)} copy(f32[64,8]{0,1:T(8,128)} %param.19) | data formatting | bytes 4096 | tf_op args[9]
  2.8 55.2 %shard_map.100 = bf16[64,2048]{1,0:T(8,128)(2,1)} custom-call(bf16[64,2048]{1,0:T(8,128)(2,1)} %tok_ref.1, f32[1,2048]{1,0:T(1,128)} %bitcast.1, s32[64,8]{1,0:T(8,128)} %copy.11.routes_ref, f32[64,8]{1,0:T(8,128)} %copy.12.rweights_ref, bf16[1,2048,512]{2,1,0:T(8,128)(2,1)} %eg_hbm.1, bf16[1,2048,512]{2,1,0:T(8,128)(2,1)} %eu_hbm.1, ...), custom_call_target="tpu_custom_call" | custom-call | flops 6845104128 | bytes 12582912 | tf_op jit(solution)/shard_map/pallas_call | solution.py:376
  58.0 1.7 %copy.14 = bf16[64,2048]{1,0:T(8,128)(2,1)} copy(bf16[64,2048]{1,0:T(8,128)(2,1)} %shard_map.100) | data formatting | bytes 524288

commit v2 on v1

--- a/solution.py
+++ b/solution.py
@@ -84,8 +84,23 @@
     return (routed + shared_out.astype(jnp.float32)).astype(jnp.bfloat16)
 
 
-RING_SENDS = ((3, 1, None), (4, 0, None), (2, 1, 0), (3, 0, 1), (1, 1, 2), (2, 0, 3), (1, 0, 5))
-LAST_IN = (6, 4)
+RING_SENDS = (
+    (3, 1, 0, None),
+    (3, 1, 1, None),
+    (4, 0, 0, None),
+    (4, 0, 1, None),
+    (2, 1, 0, 0),
+    (2, 1, 1, 1),
+    (3, 0, 0, 2),
+    (3, 0, 1, 3),
+    (1, 1, 0, 4),
+    (2, 0, 0, 6),
+    (2, 0, 1, 7),
+    (1, 1, 1, 5),
+    (1, 0, 0, 9),
+    (1, 0, 1, 10),
+)
+LAST_IN = ((12, 13), (8, 11))
 
 
 def remote(src, dst, send_sem, recv_sem, target):
@@ -138,6 +153,7 @@
 ):
     width = tok_ref.shape[1]
     quarter = tok_ref.shape[0] // 2
+    eighth = quarter // 2
     block = 4 * quarter
     experts = 2 * chips
     depth = chips // 2
@@ -180,12 +196,14 @@
     scaled = wide * lax.rsqrt(jnp.mean(wide * wide, axis=-1, keepdims=True) + 1e-06)
     normed = (scaled * gain_ref[...]).astype(jnp.bfloat16)
     rows[0, core, :, :, :width] = normed.reshape(2, quarter, width)
+    named = lax.rem(lax.broadcasted_iota(jnp.int32, (128, 2 * quarter), 0), experts)
+    table = jnp.zeros((128, 2 * quarter), jnp.float32)
+    for k in range(routes_ref.shape[0]):
+        table = table + jnp.where(
+            named == routes_ref[k : k + 1, :], rweights_ref[k : k + 1, :], 0.0
+        )
+    table = table.T
     lane = lax.broadcasted_iota(jnp.int32, (2 * quarter, 128), 1)
-    table = jnp.zeros((2 * quarter, 128), jnp.float32)
-    for k in range(routes_ref.shape[1]):
-        table = table + jnp.where(
-            lax.rem(lane, experts) == routes_ref[:, k : k + 1], rweights_ref[:, k : k + 1], 0.0
-        )
     coarse = table.astype(jnp.bfloat16).astype(jnp.float32)
     table = jnp.where(lane < experts, coarse, jnp.where(lane < 2 * experts, table - coarse, 0.0))
     rows[0, core, :, :, width:] = table.astype(jnp.bfloat16).reshape(2, quarter, 128)
@@ -244,7 +262,7 @@
                 hid[...], ed[:, lower : lower + step], preferred_element_type=jnp.float32
             )
             part[slot, :, :, :, lower : lower + step] = (
-                (o * weight).astype(jnp.bfloat16).reshape(2, 2, quarter, step)
+                (o * weight).astype(jnp.bfloat16).reshape(2, 4, eighth, step)
             )
         mate_copy(slot).start()
 
@@ -282,7 +300,10 @@
         expert_block(u)
         return carry
 
-    lax.fori_loop(0, chips - 1, gather_step, 0)
+    lax.fori_loop(0, last, gather_step, 0)
+    for k in (last - 2, last - 1):
+        across_copy(1, k).wait_recv()
+    expert_block(last)
 
     mate_seen = set()
 
@@ -292,26 +313,31 @@
         )
 
     def ring_send(way, k):
-        hops, kind, inbound = RING_SENDS[k]
+        hops, kind, piece, inbound = RING_SENDS[k]
         slot = min(2 * hops, chips - 1) if way == 0 else 2 * hops - 1
-        half = kind if way == 0 else 1 - kind
+        piece = 2 * (kind if way == 0 else 1 - kind) + piece
         if slot not in mate_seen:
             mate_copy(slot).wait_recv()
             mate_seen.add(slot)
-        total = part[slot, core, half].astype(jnp.float32) + mate[slot, half].astype(jnp.float32)
+        total = part[slot, core, piece].astype(jnp.float32) + mate[slot, piece].astype(jnp.float32)
         if inbound is not None:
             ring_copy(way, inbound).wait_recv()
             total = total + rbuf[way, inbound].astype(jnp.float32)
         sbuf[way, k] = total.astype(jnp.bfloat16)
         ring_copy(way, k).start()
 
-    ring_send(1, 0)
+    for way in (1, 0):
+        for k in (0, 1):
+            ring_send(way, k)
+    for way in (0, 1):
+        arrival(way, last).wait_recv()
+        across_copy(way, last).start()
     for way in (0, 1):
         across_copy(way, last).wait_recv()
     expert_block(chips - 1)
-    ring_send(0, 0)
     for way in (0, 1):
-        ring_send(way, 1)
+        for k in (2, 3):
+            ring_send(way, k)
 
     for load in loads[3:]:
         load.wait()
@@ -323,28 +349,30 @@
         )
         cut = slice(lower, lower + step)
         shared[:, :, cut] = (
-            o.astype(jnp.bfloat16).astype(jnp.float32).reshape(2, quarter, step)
+            o.astype(jnp.bfloat16).astype(jnp.float32).reshape(4, eighth, step)
             + part[0, core, :, :, cut].astype(jnp.float32)
             + mate[0, :, :, cut].astype(jnp.float32)
         )
 
-    for k in range(2, len(RING_SENDS)):
+    for k in range(4, len(RING_SENDS)):
         for way in (0, 1):
             ring_send(way, k)
 
-    for half in (1, 0):
-        total = shared[half]
+    for piece in (0, 1, 2, 3):
+        total = shared[piece]
         for way in (0, 1):
-            k = LAST_IN[half if way == 0 else 1 - half]
+            half = piece // 2 if way == 0 else 1 - piece // 2
+            k = LAST_IN[half][piece % 2]
             ring_copy(way, k).wait_recv()
             total = total + rbuf[way, k].astype(jnp.float32)
-        out_ref[half * quarter : (half + 1) * quarter, :] = total.astype(jnp.bfloat16)
+        out_ref[piece * eighth : (piece + 1) * eighth, :] = total.astype(jnp.bfloat16)
 
     own_copy.wait_send()
     for way in (0, 1):
         for k in range(last + 1):
             gather_copy(way, k, k < 2).wait_send()
             across_copy(way, k).wait_send()
+        for k in range(len(RING_SENDS)):
             ring_copy(way, k).wait_send()
     for slot in range(chips):
         mate_copy(slot).wait_send()
@@ -369,6 +397,7 @@
     hidden = expert_gate.shape[2]
     half = jnp.bfloat16
     messages = chips - 1
+    sends = len(RING_SENDS)
     whole = pl.BlockSpec(memory_space=pltpu.VMEM)
     stays = pl.BlockSpec(memory_space=pl.ANY)
     dma = pltpu.SemaphoreType.DMA
@@ -380,8 +409,8 @@
         out_specs=whole,
         scratch_shapes=[
             pltpu.VMEM((chips, 2, 2, quarter, width + 128), half),
-            pltpu.VMEM((chips, 2, 2, quarter, width), half),
-            pltpu.VMEM((chips, 2, quarter, width), half),
+            pltpu.VMEM((chips, 2, 4, quarter // 2, width), half),
+            pltpu.VMEM((chips, 4, quarter // 2, width), half),
             pltpu.VMEM((2 * count, hidden), half),
             pltpu.VMEM((width, hidden), half),
             pltpu.VMEM((width, hidden), half),
@@ -389,9 +418,9 @@
             pltpu.VMEM((width, hidden), half),
             pltpu.VMEM((width, hidden), half),
             pltpu.VMEM((hidden, width), half),
-            pltpu.VMEM((2, messages, quarter, width), half),
-            pltpu.VMEM((2, messages, quarter, width), half),
-            pltpu.VMEM((2, quarter, width), jnp.float32),
+            pltpu.VMEM((2, sends, quarter // 2, width), half),
+            pltpu.VMEM((2, sends, quarter // 2, width), half),
+            pltpu.VMEM((4, quarter // 2, width), jnp.float32),
             dma((6,)),
             dma((2,)),
             dma((2, messages)),
@@ -400,8 +429,8 @@
             dma((2, messages)),
             dma((chips,)),
             dma((chips,)),
-            dma((2, messages)),
-            dma((2, messages)),
+            dma((2, sends)),
+            dma((2, sends)),
         ],
         compiler_params=pltpu.CompilerParams(
             collective_id=0, has_side_effects=True, vmem_limit_bytes=60 * 2**20
@@ -412,8 +441,8 @@
     )(
         tokens,
         norm_gain.reshape(1, width),
-        routes,
-        route_weights,
+        routes.T,
+        route_weights.T,
         expert_gate,
         expert_up,
         expert_down,

time: 59.9 us -> 56.6 us (0.945)
  local copies, waits for them, and re-layouts: 4.42 us -> 1.67 us
    unnamed x3 -> x1, local copies, waits for them, and re-layouts: 4.42 us -> 1.67 us
where the time goes in v2:
time: 56.6 us; the launch traced here: 56.5 us
  Pallas kernels  54.8 us (97%)
  local copies, waits for them, and re-layouts  1.67 us (3%)
    pallas_call x1, Pallas kernels, ring_per_device(): pl.pallas_call(functools.partial(moe_kernel, chips), out_shape=jax.ShapeD...  54.8 us
    unnamed x1, local copies, waits for them, and re-layouts  1.67 us

profile of v2, /device:TPU:0, one launch (start us, length us, event | category | flops | bytes accessed | tf_op | source)
XLA Modules:
  0.0 56.5 jit_solution(7247214459582869867)
XLA Ops:
  0.0 54.8 %shard_map.100 = bf16[64,2048]{1,0:T(8,128)(2,1)} custom-call(bf16[64,2048]{1,0:T(8,128)(2,1)} %tok_ref.1, f32[1,2048]{1,0:T(1,128)} %bitcast.3, s32[8,64]{1,0:T(8,128)} %bitcast.4, f32[8,64]{1,0:T(8,128)} %bitcast.5, bf16[1,2048,512]{2,1,0:T(8,128)(2,1)} %eg_hbm.1, bf16[1,2048,512]{2,1,0:T(8,128)(2,1)} %eu_hbm.1, bf16[1,512,2048]{2,1,0:T(8,128)(2,1)} %ed_hbm.1, ...), custom_call_target="tpu_custom_call" | custom-call | flops 6845104128 | bytes 12582912 | tf_op jit(solution)/shard_map/pallas_call | solution.py:405
  54.8 1.7 %copy.12 = bf16[64,2048]{1,0:T(8,128)(2,1)} copy(bf16[64,2048]{1,0:T(8,128)(2,1)} %shard_map.100) | data formatting | bytes 524288

commit v3 on v2

--- a/solution.py
+++ b/solution.py
@@ -128,6 +128,7 @@
     sd_hbm,
     out_ref,
     rows,
+    tables,
     part,
     mate,
     hid,
@@ -146,6 +147,10 @@
     ag_recv,
     dd_send,
     dd_recv,
+    tg_send,
+    tg_recv,
+    td_send,
+    td_recv,
     y_send,
     y_recv,
     rs_send,
@@ -195,18 +200,17 @@
     wide = tok_ref[...].astype(jnp.float32)
     scaled = wide * lax.rsqrt(jnp.mean(wide * wide, axis=-1, keepdims=True) + 1e-06)
     normed = (scaled * gain_ref[...]).astype(jnp.bfloat16)
-    rows[0, core, :, :, :width] = normed.reshape(2, quarter, width)
-    named = lax.rem(lax.broadcasted_iota(jnp.int32, (128, 2 * quarter), 0), experts)
-    table = jnp.zeros((128, 2 * quarter), jnp.float32)
+    rows[0, core] = normed.reshape(2, quarter, width)
+    tally = 2 * quarter
+    named = lax.broadcasted_iota(jnp.int32, (experts, 2 * tally), 0)
+    twice = jnp.concatenate([routes_ref[...], routes_ref[...]], axis=1)
+    worth = jnp.concatenate([rweights_ref[...], rweights_ref[...]], axis=1)
+    table = jnp.zeros((experts, 2 * tally), jnp.float32)
     for k in range(routes_ref.shape[0]):
-        table = table + jnp.where(
-            named == routes_ref[k : k + 1, :], rweights_ref[k : k + 1, :], 0.0
-        )
-    table = table.T
-    lane = lax.broadcasted_iota(jnp.int32, (2 * quarter, 128), 1)
+        table = table + jnp.where(named == twice[k : k + 1, :], worth[k : k + 1, :], 0.0)
     coarse = table.astype(jnp.bfloat16).astype(jnp.float32)
-    table = jnp.where(lane < experts, coarse, jnp.where(lane < 2 * experts, table - coarse, 0.0))
-    rows[0, core, :, :, width:] = table.astype(jnp.bfloat16).reshape(2, quarter, 128)
+    lane = lax.broadcasted_iota(jnp.int32, (experts, 2 * tally), 1)
+    tables[0, core] = jnp.where(lane < tally, coarse, table - coarse).astype(jnp.bfloat16)
     pl.semaphore_wait(barrier, 3)
 
     def spot_of(way, k):
@@ -230,16 +234,38 @@
         ref = spot_of(way, k)
         return remote(ref, ref, dd_send.at[way, k], dd_recv.at[way, k], partner)
 
+    def table_at(way, hops):
+        return tables.at[2 * hops - 1 if way == 0 else 2 * hops, core]
+
+    def table_copy(way, hops, source):
+        return remote(
+            source,
+            table_at(way, hops),
+            tg_send.at[way, hops - 1],
+            tg_recv.at[way, hops - 1],
+            ahead[way],
+        )
+
+    def table_across(way, hops):
+        ref = table_at(way, hops)
+        return remote(ref, ref, td_send.at[way, hops - 1], td_recv.at[way, hops - 1], partner)
+
     def mate_copy(slot):
         return remote(
             part.at[slot, 1 - core], mate.at[slot], y_send.at[slot], y_recv.at[slot], partner
         )
 
+    for way in (0, 1):
+        table_copy(way, 1, tables.at[0, core]).start()
     for k in (0, 1):
         for way in (0, 1):
             gather_copy(way, k, True).start()
     own_copy = remote(rows.at[0, core], rows.at[0, core], own_sem.at[0], own_sem.at[1], partner)
     own_copy.start()
+    own_table = remote(
+        tables.at[0, core], tables.at[0, core], own_sem.at[2], own_sem.at[3], partner
+    )
+    own_table.start()
 
     step = 256
 
@@ -250,12 +276,12 @@
             hid[:count, lower : lower + step] = (jax.nn.silu(g) * u).astype(jnp.bfloat16)
 
     def expert_block(slot):
-        x = rows[slot, :, :, :, :width].reshape(block, width)
-        extra = rows[slot, :, :, :, width:].reshape(block, 128).astype(jnp.float32)
-        where = lax.broadcasted_iota(jnp.int32, (block, 128), 1)
-        weight = jnp.sum(
-            jnp.where((where == me) | (where == me + experts), extra, 0.0), axis=1, keepdims=True
-        )
+        x = rows[slot].reshape(block, width)
+        mine = lax.broadcasted_iota(jnp.int32, (2, experts, 2 * tally), 1) == me
+        lines = jnp.sum(jnp.where(mine, tables[slot].astype(jnp.float32), 0.0), axis=1)
+        lines = lines[:, :tally] + lines[:, tally:]
+        line = jnp.concatenate([lines[0:1], lines[1:2]], axis=1)
+        weight = jnp.broadcast_to(line, (8, block)).T[:, 0:1]
         hidden_of(x, eg, eu, block)
         for lower in range(0, width, step):
             o = jnp.dot(
@@ -272,6 +298,19 @@
     last = chips - 2
 
     def gather_step(u, carry):
+        hops = 1 + u // 2
+
+        @pl.when(u % 2 == 0)
+        def _():
+            for way in (0, 1):
+                table_copy(way, hops, table_at(way, hops)).wait_recv()
+                table_across(way, hops).start()
+            table_copy(0, hops + 1, table_at(0, hops)).start()
+
+            @pl.when(hops < depth - 1)
+            def _():
+                table_copy(1, hops + 1, table_at(1, hops)).start()
+
         for way in (0, 1):
             arrival(way, u).wait_recv()
 
@@ -284,6 +323,7 @@
         @pl.when(u == 0)
         def _():
             own_copy.wait_recv()
+            own_table.wait_recv()
 
         first = 2 * ((u + 1) // 2 - 1)
 
@@ -291,11 +331,13 @@
         def _():
             across_copy(0, first).wait_recv()
             across_copy(0, first + 1).wait_recv()
+            table_across(0, 1 + first // 2).wait_recv()
 
         @pl.when((u > 0) & (u % 2 == 0))
         def _():
             across_copy(1, first).wait_recv()
             across_copy(1, first + 1).wait_recv()
+            table_across(1, 1 + first // 2).wait_recv()
 
         expert_block(u)
         return carry
@@ -303,6 +345,7 @@
     lax.fori_loop(0, last, gather_step, 0)
     for k in (last - 2, last - 1):
         across_copy(1, k).wait_recv()
+    table_across(1, depth - 1).wait_recv()
     expert_block(last)
 
     mate_seen = set()
@@ -329,11 +372,14 @@
     for way in (1, 0):
         for k in (0, 1):
             ring_send(way, k)
+    table_copy(0, depth, table_at(0, depth)).wait_recv()
+    table_across(0, depth).start()
     for way in (0, 1):
         arrival(way, last).wait_recv()
         across_copy(way, last).start()
     for way in (0, 1):
         across_copy(way, last).wait_recv()
+    table_across(0, depth).wait_recv()
     expert_block(chips - 1)
     for way in (0, 1):
         for k in (2, 3):
@@ -341,7 +387,7 @@
 
     for load in loads[3:]:
         load.wait()
-    hidden_of(rows[0, core, :, :, :width].reshape(2 * quarter, width), sg, su, 2 * quarter)
+    hidden_of(rows[0, core].reshape(2 * quarter, width), sg, su, 2 * quarter)
     mate_copy(0).wait_recv()
     for lower in range(0, width, step):
         o = jnp.dot(
@@ -368,6 +414,11 @@
         out_ref[piece * eighth : (piece + 1) * eighth, :] = total.astype(jnp.bfloat16)
 
     own_copy.wait_send()
+    own_table.wait_send()
+    for way in (0, 1):
+        for hops in range(1, depth + 1 - way):
+            table_copy(way, hops, tables.at[0, core]).wait_send()
+            table_across(way, hops).wait_send()
     for way in (0, 1):
         for k in range(last + 1):
             gather_copy(way, k, k < 2).wait_send()
@@ -408,7 +459,8 @@
         in_specs=[whole] * 4 + [stays] * 6,
         out_specs=whole,
         scratch_shapes=[
-            pltpu.VMEM((chips, 2, 2, quarter, width + 128), half),
+            pltpu.VMEM((chips, 2, 2, quarter, width), half),
+            pltpu.VMEM((chips, 2, experts, 2 * count), half),
             pltpu.VMEM((chips, 2, 4, quarter // 2, width), half),
             pltpu.VMEM((chips, 4, quarter // 2, width), half),
             pltpu.VMEM((2 * count, hidden), half),
@@ -422,11 +474,15 @@
             pltpu.VMEM((2, sends, quarter // 2, width), half),
             pltpu.VMEM((4, quarter // 2, width), jnp.float32),
             dma((6,)),
-            dma((2,)),
+            dma((4,)),
             dma((2, messages)),
             dma((2, messages)),
             dma((2, messages)),
             dma((2, messages)),
+            dma((2, chips // 2)),
+            dma((2, chips // 2)),
+            dma((2, chips // 2)),
+            dma((2, chips // 2)),
             dma((chips,)),
             dma((chips,)),
             dma((2, sends)),

time: 56.6 us -> 55.9 us (0.988)
  Pallas kernels: 54.8 us -> 54.1 us
    pallas_call x1, Pallas kernels: 54.8 us -> 54.1 us  [ring_per_device(): pl.pallas_call(functools.partial(moe_kernel, chips), out_shape=jax.ShapeD...]
where the time goes in v3:
time: 55.9 us; the launch traced here: 55.7 us
  Pallas kernels  54.1 us (97%)
  local copies, waits for them, and re-layouts  1.67 us (3%)
    pallas_call x1, Pallas kernels, ring_per_device(): pl.pallas_call(functools.partial(moe_kernel, chips), out_shape=jax.ShapeD...  54.1 us
    unnamed x1, local copies, waits for them, and re-layouts  1.67 us

profile of v3, /device:TPU:0, one launch (start us, length us, event | category | flops | bytes accessed | tf_op | source)
XLA Modules:
  0.0 55.7 jit_solution(13295599606306128693)
XLA Ops:
  0.0 54.1 %shard_map.100 = bf16[64,2048]{1,0:T(8,128)(2,1)} custom-call(bf16[64,2048]{1,0:T(8,128)(2,1)} %tok_ref.1, f32[1,2048]{1,0:T(1,128)} %bitcast.3, s32[8,64]{1,0:T(8,128)} %bitcast.4, f32[8,64]{1,0:T(8,128)} %bitcast.5, bf16[1,2048,512]{2,1,0:T(8,128)(2,1)} %eg_hbm.1, bf16[1,2048,512]{2,1,0:T(8,128)(2,1)} %eu_hbm.1, bf16[1,512,2048]{2,1,0:T(8,128)(2,1)} %ed_hbm.1, ...), custom_call_target="tpu_custom_call" | custom-call | flops 6845104128 | bytes 12582912 | tf_op jit(solution)/shard_map/pallas_call | solution.py:456
  54.1 1.7 %copy.12 = bf16[64,2048]{1,0:T(8,128)(2,1)} copy(bf16[64,2048]{1,0:T(8,128)(2,1)} %shard_map.100) | data formatting | bytes 524288
